TPU v7x, 512 devices: a whole 4x8x8 slice. The times are simulated.
512 devices in a mesh: sp: 32 (over z, x), tp: 16 (over y, core).
Axes of the slice: x: 4, y: 8, z: 8, core: 2. Of those that a mesh axis runs over, the one named last changes fastest.
Arguments:
- residual: bfloat16 [8192, 2048], P('sp', 'tp'), may hold values from -6 to 6
- queries: bfloat16 [8192, 1024], P('sp', 'tp'), may hold values from -5.5 to 5.5
- keys: bfloat16 [8192, 128], P('sp'), may hold values from -5.5 to 5.5
- values: bfloat16 [8192, 128], P('sp'), may hold values from -6 to 6
- documents: int32 [8192], P('sp'), may hold values from 0 to 15, never falling along the last dimension, each value on 1 to 1024 neighbouring positions
- sinks: float32 [16], P('tp'), may hold values from 1 to 6
- head_gain: float32 [1024], replicated, may hold values from 0.1 to 1.9
- out_weight: bfloat16 [1024, 2048], P(None, 'tp'), may hold values from -0.1875 to 0.1875
- norm_gain: float32 [2048], P('tp'), may hold values from 0.1 to 1.9
- norm_shift: float32 [2048], P('tp'), may hold values from -3 to 3
- routes: int32 [8192, 2], P('sp'), may hold values from 0 to 31, all different within a row; in each aligned block of 256 rows (0 to 255, 256 to 511, ...) at most 24 rows name the same one
- route_logits: float32 [8192, 2], P('sp'), may hold values from -150 to 150
- gate_weight: bfloat16 [32, 2048, 6144], P('sp', None, 'tp'), may hold values from -0.125 to 0.125
- up_weight: bfloat16 [32, 2048, 6144], P('sp', None, 'tp'), may hold values from -0.125 to 0.125
- down_weight: bfloat16 [32, 6144, 2048], P('sp', 'tp'), may hold values from -0.15625 to 0.15625
- final_gain: float32 [2048], P('tp'), may hold values from 0.1 to 1.9
- final_shift: float32 [2048], P('tp'), may hold values from -3 to 3
Outputs:
- layer_out: bfloat16 [8192, 2048], P('sp', 'tp')
Inputs may be any that keep to these rules, and one draw needn't show every extreme that they name: `documents`: document numbers never fall along the sequence; each document has at least one position and at most 1024, and some document has exactly 1024. `routes`: each row names 2 different experts. In each aligned block of 256 rows (the rows of one index of sp) no expert is named by more than 24 rows, a bound that some block reaches.
All inputs are finite; a program needn't handle non-finite values.
Results may differ from a plain program's by a relative error of at most 0.014.
Values may be sent and summed in bfloat16 or wider, within the bound.
A program may use at most 128 MiB of HBM per device.

v0:
```python
import jax
import jax.numpy as jnp
from jax import lax
from jax.sharding import PartitionSpec as P

D = 2048
QUERY_HEADS = 16
KEY_VALUE_HEADS = 2
HEAD_SIZE = 64
WINDOW_SIZE = 128
TOP = 2
DEEP_ALPHA = 8.0**0.25
NORM_EPS = 1e-05


def sent_to_all(value, axis):
    length = lax.axis_size(axis)
    return lax.all_to_all(
        jnp.broadcast_to(value[None], (length, *value.shape)), axis, 0, 0, tiled=True
    )


def over_copies(value, axis):
    return sent_to_all(value, axis).sum(axis=0)


def in_one(arrays, axis):
    line, at, gathered = (jnp.concatenate([a.reshape(-1) for a in arrays]), 0, [])
    total = over_copies(line, axis)
    for a in arrays:
        gathered.append(total[at : at + a.size].reshape(a.shape))
        at += a.size
    return tuple(gathered)


def shifted(block, axis, distance):
    devices = range(lax.axis_size(axis))
    route = [(i - distance, i) for i in devices if i - distance in devices]
    return lax.ppermute(block, axis, route)


def split_norm(total, gain, shift):
    totals = in_one((jnp.sum(total, axis=1), jnp.sum(total * total, axis=1)), "tp")
    center = totals[0] / D
    spread = totals[1] / D - center * center
    return (total - center[:, None]) * lax.rsqrt(spread + NORM_EPS)[:, None] * gain + shift


def expert_rows(arrived, gate_weight, up_weight, down_weight):
    sources, count, width = arrived.shape
    flat_rows = arrived.reshape(sources * count, width)
    gate = jnp.dot(flat_rows, gate_weight[0], preferred_element_type=jnp.float32)
    up_val = jnp.dot(flat_rows, up_weight[0], preferred_element_type=jnp.float32)
    middle = (jax.nn.silu(gate) * up_val).astype(jnp.bfloat16)
    share_out = jnp.dot(middle, down_weight[0], preferred_element_type=jnp.float32).astype(
        jnp.bfloat16
    )
    groups = lax.axis_size("tp")
    pieces = share_out.reshape(sources, count, groups, width // groups)
    traded = lax.all_to_all(pieces, "tp", split_axis=2, concat_axis=2, tiled=True)
    summed = jnp.sum(traded.astype(jnp.float32), axis=2)
    return lax.all_to_all(
        summed.astype(jnp.bfloat16), "sp", split_axis=0, concat_axis=0, tiled=True
    )


def pack_rows(source_rows, table, expert_count, capacity):
    padded = jnp.concatenate(
        [source_rows, jnp.zeros((1, source_rows.shape[1]), source_rows.dtype)], axis=0
    )
    return padded[table].reshape(expert_count, capacity, source_rows.shape[1])


def local(
    residual,
    queries,
    keys,
    values,
    documents,
    sinks,
    head_gain,
    out_weight,
    norm_gain,
    norm_shift,
    routes,
    route_logits,
    gate_weight,
    up_weight,
    down_weight,
    final_gain,
    final_shift,
):
    tokens = queries.shape[0]
    head_list = sinks.shape[0]
    tails = shifted(
        (
            keys[tokens - WINDOW_SIZE :],
            values[tokens - WINDOW_SIZE :],
            documents[tokens - WINDOW_SIZE :].astype(jnp.bfloat16),
        ),
        "sp",
        1,
    )
    offset = lax.axis_index("sp") * tokens
    shared_key_head = lax.axis_index("tp") * head_list // (QUERY_HEADS // KEY_VALUE_HEADS)
    all_keys = jnp.concatenate([tails[0], keys], axis=0)
    all_values = jnp.concatenate([tails[1], values], axis=0)
    all_docs = jnp.concatenate([tails[2].astype(jnp.int32), documents], axis=0)
    key_head = lax.dynamic_slice_in_dim(all_keys, shared_key_head * HEAD_SIZE, HEAD_SIZE, 1)
    value_head = lax.dynamic_slice_in_dim(all_values, shared_key_head * HEAD_SIZE, HEAD_SIZE, 1)
    query_heads = queries.reshape(tokens, head_list, HEAD_SIZE)
    scores = jnp.einsum(
        "qhd,kd->hqk", query_heads, key_head, preferred_element_type=jnp.float32
    ) * HEAD_SIZE ** (-0.5)
    query_pos = offset + jnp.arange(tokens, dtype=jnp.int32)
    key_pos = offset - WINDOW_SIZE + jnp.arange(tokens + WINDOW_SIZE, dtype=jnp.int32)
    distance = query_pos[:, None] - key_pos[None, :]
    allowed = (
        (distance >= 0)
        & (distance < WINDOW_SIZE)
        & (key_pos[None, :] >= 0)
        & (documents[:, None] == all_docs[None, :])
    )
    scores = jnp.where(allowed[None], scores, -jnp.inf)
    sink_col = sinks[:, None]
    top = jnp.maximum(jnp.max(scores, axis=2), sink_col)
    expd = jnp.exp(scores - top[..., None])
    probs = (expd / (jnp.sum(expd, axis=2) + jnp.exp(sink_col - top))[..., None]).astype(
        jnp.bfloat16
    )
    attended = jnp.einsum("hqk,kd->qhd", probs, value_head, preferred_element_type=jnp.float32)
    attended = attended.astype(jnp.bfloat16).reshape(tokens, head_list * HEAD_SIZE)
    all_heads = lax.all_gather(attended, "tp", axis=1, tiled=True).astype(jnp.float32)
    scaled = (
        all_heads
        * lax.rsqrt(jnp.mean(all_heads * all_heads, axis=1, keepdims=True) + NORM_EPS)
        * head_gain
    ).astype(jnp.bfloat16)
    mix = jnp.dot(scaled, out_weight, preferred_element_type=jnp.float32)
    first = DEEP_ALPHA * residual.astype(jnp.float32) + mix
    hidden = split_norm(first, norm_gain, norm_shift)
    hidden_rows = hidden.astype(jnp.bfloat16)
    expert_count = lax.axis_size("sp")
    capacity = 3 * tokens * TOP // (2 * expert_count)
    flat = routes.reshape(-1)
    onehot = (flat[:, None] == jnp.arange(expert_count, dtype=jnp.int32)[None, :]).astype(jnp.int32)
    rank = jnp.sum(jnp.cumsum(onehot, axis=0) * onehot, axis=1) - 1
    target = flat * capacity + rank
    owner = jnp.arange(tokens * TOP, dtype=jnp.int32) // TOP
    table = jnp.full((expert_count * capacity,), tokens, jnp.int32).at[target].set(owner)
    outgoing = pack_rows(hidden_rows, table, expert_count, capacity)
    joined = lax.all_gather(
        lax.all_to_all(outgoing, "sp", split_axis=0, concat_axis=0, tiled=True),
        "tp",
        axis=2,
        tiled=True,
    )
    returned = expert_rows(joined, gate_weight, up_weight, down_weight)
    picked = (
        returned.reshape(expert_count * capacity, -1)[target]
        .reshape(tokens, TOP, -1)
        .astype(jnp.float32)
    )
    share = jax.nn.softmax(route_logits, axis=-1)
    moe = jnp.sum(share[:, :, None] * picked, axis=1)
    second = DEEP_ALPHA * hidden + moe
    return split_norm(second, final_gain, final_shift).astype(jnp.bfloat16)


def solution(mesh):
    return jax.shard_map(
        local,
        mesh=mesh,
        in_specs=(
            P("sp", "tp"),
            P("sp", "tp"),
            P("sp", None),
            P("sp", None),
            P("sp"),
            P("tp"),
            P(),
            P(None, "tp"),
            P("tp"),
            P("tp"),
            P("sp", None),
            P("sp", None),
            P("sp", None, "tp"),
            P("sp", None, "tp"),
            P("sp", "tp", None),
            P("tp"),
            P("tp"),
        ),
        out_specs=P("sp", "tp"),
        check_vma=False,
    )
```

profile of v0, /device:TPU:1, one launch (start us, length us, event | category | flops | bytes accessed | tf_op | source)
XLA Modules:
  0.0 268.2 jit_solution(7688286295900288744)
XLA Ops:
  6.5 0.9 slice.30
  7.4 3.9 %collective-permute-start.2 = (bf16[128,128]{1,0:T(8,128)(2,1)S(1)}, bf16[128,128]{1,0:T(8,128)(2,1)S(1)}, u32[]{:S(2)}, u32[]{:S(2)}) collective-permute-start(bf16[128,128]{1,0:T(8,128)(2,1)S(1)} %slice.30), channel_id=1, source_target_pairs={{0,16},{16,32},{32,48},{48,64},{64,80},{80,96},{96,112},{112,128},... | collective-permute-start | bytes 98312 | tf_op jit(solution)/shard_map/ppermute | solution.py:39
  11.4 0.7 convert.5
  12.0 3.1 %collective-permute-start.1 = (bf16[128]{0:T(256)(128)(2,1)S(1)}, bf16[128]{0:T(256)(128)(2,1)S(1)}, u32[]{:S(2)}, u32[]{:S(2)}) collective-permute-start(bf16[128]{0:T(256)(128)(2,1)S(1)} %slice.29), channel_id=1, source_target_pairs={{0,16},{16,32},{32,48},{48,64},{64,80},{80,96},{96,112},{112,128},... | collective-permute-start | bytes 776 | tf_op jit(solution)/shard_map/ppermute | solution.py:39
  15.2 0.8 slice.28
  15.9 2.8 %collective-permute-start = (bf16[128,128]{1,0:T(8,128)(2,1)S(1)}, bf16[128,128]{1,0:T(8,128)(2,1)S(1)}, u32[]{:S(2)}, u32[]{:S(2)}) collective-permute-start(bf16[128,128]{1,0:T(8,128)(2,1)S(1)} %slice.28), channel_id=1, source_target_pairs={{0,16},{16,32},{32,48},{48,64},{64,80},{80,96},{96,112},{112,128},... | collective-permute-start | bytes 98312 | tf_op jit(solution)/shard_map/ppermute | solution.py:39
  18.8 0.8 copy.39
  19.9 0.7 broadcast_multiply_fusion
  20.6 1.2 reduce-window.6
  22.5 2.4 scatter_custom_fusion
  25.6 0.7 pad_add_fusion
  26.3 1.2 fusion.55
  28.0 20.4 %all-gather = bf16[256,1,1024]{0,2,1:T(8,128)(2,1)S(1)} all-gather(bf16[256,1,64]{0,2,1:T(8,128)(2,1)S(1)} %fusion.14), channel_id=2, replica_groups=mesh['sp'=32,'tp'=16] {'tp'}, dimensions={2}, use_global_device_ids=true | all-gather | bytes 557056 | tf_op jit(solution)/shard_map/all_gather | solution.py:133
  48.6 0.7 fusion.54
  49.2 0.6 broadcast_in_dim.13
  49.9 4.5 %all-to-all-start = ((f32[16,1,512]{2,1,0:T(1,128)}), f32[16,1,512]{2,1,0:T(1,128)S(1)}, u32[]{:S(2)}, u32[]{:S(2)}) async-start(f32[16,1,512]{2,1,0:T(1,128)} %broadcast_in_dim.13), calls=%async_computation | async-start | bytes 65536 | tf_op jit(solution)/shard_map/all_to_all | solution.py:18
  54.4 7.3 %all-to-all-done = f32[16,1,512]{2,1,0:T(1,128)S(1)} async-done(((f32[16,1,512]{2,1,0:T(1,128)}), f32[16,1,512]{2,1,0:T(1,128)S(1)}, u32[]{:S(2)}, u32[]{:S(2)}) %all-to-all-start) | async-done | bytes 32800 | tf_op jit(solution)/shard_map/all_to_all | solution.py:18
  62.0 1.9 gather_fusion
  63.9 23.3 %all_to_all.27 = bf16[32,24,128]{2,1,0:T(8,128)(2,1)} all-to-all(bf16[32,24,128]{2,1,0:T(8,128)(2,1)S(1)} %bitcast.72), channel_id=1, replica_groups=mesh['sp'=32,'tp'=16] {'sp'}, dimensions={0} | all-to-all | bytes 393216 | tf_op jit(solution)/shard_map/all_to_all | solution.py:153
  87.2 39.9 %all-gather.3.cloned.1.call-done = bf16[32,24,2048]{2,1,0:T(8,128)(2,1)} async-done(((bf16[32,24,128]{2,1,0:T(8,128)(2,1)}), bf16[32,24,2048]{2,1,0:T(8,128)(2,1)}) %all-gather.3.cloned.1.call-update) | async-done | bytes 3145744 | tf_op jit(solution)/shard_map/all_gather | solution.py:152
  127.1 5.3 %fusion.4 = f32[768,384]{1,0:T(8,128)} fusion(bf16[768,2048]{1,0:T(8,128)(2,1)} %bitcast.77, bf16[1,2048,384]{2,1,0:T(8,128)(2,1)} %param.29), kind=kOutput, calls=%fused_computation.8 | convolution fusion | flops 1207959552 | bytes 5898240 | tf_op jit(solution)/shard_map/dot_general | solution.py:52
  132.4 7.4 %fusion = bf16[96,8,16,128]{3,1,2,0:T(8,128)(2,1)} fusion(bf16[1,384,2048]{2,1,0:T(8,128)(2,1)S(1)} %copy-done, bf16[768,2048]{1,0:T(8,128)(2,1)} %bitcast.78, bf16[1,2048,384]{2,1,0:T(8,128)(2,1)S(1)} %copy-done.7, f32[768,384]{1,0:T(8,128)} %fusion.4), kind=kOutput, calls=%fused_computation.4 | convolution fusion | flops 2419261440 | bytes 10616832 | tf_op jit(solution)/shard_map/dot_general | solution.py:55
  139.7 2.9 %copy.51 = bf16[96,8,16,128]{3,2,1,0:T(8,128)(2,1)S(1)} copy(bf16[96,8,16,128]{3,1,2,0:T(8,128)(2,1)} %fusion) | data formatting | bytes 6291456
  142.6 2.5 copy.42
  145.2 4.6 %all-to-all-start.2 = ((bf16[32,24,16,128]{3,1,0,2:T(8,128)(2,1)}), bf16[32,24,16,128]{3,1,0,2:T(8,128)(2,1)}, u32[]{:S(2)}, u32[]{:S(2)}) async-start(bf16[32,24,16,128]{3,1,0,2:T(8,128)(2,1)} %copy.42), calls=%async_computation.2 | async-start | bytes 6291456 | tf_op jit(solution)/shard_map/all_to_all | solution.py:60
  149.8 71.1 %all-to-all-done.2 = bf16[32,24,16,128]{3,1,0,2:T(8,128)(2,1)} async-done(((bf16[32,24,16,128]{3,1,0,2:T(8,128)(2,1)}), bf16[32,24,16,128]{3,1,0,2:T(8,128)(2,1)}, u32[]{:S(2)}, u32[]{:S(2)}) %all-to-all-start.2) | async-done | bytes 3145760 | tf_op jit(solution)/shard_map/all_to_all | solution.py:60
  220.9 3.1 %reduce_sum.118 = bf16[32,24,128]{2,1,0:T(8,128)(2,1)} reduce(bf16[32,24,16,128]{3,1,0,2:T(8,128)(2,1)} %all-to-all-done.2, bf16[]{:T(256)} %constant.87.clone.1), dimensions={2}, to_apply=%region_12.13 | reduce | flops 1474560 | bytes 3342338 | tf_op jit(solution)/shard_map/reduce_sum | solution.py:61
  223.9 9.7 %all-to-all-start.3 = ((bf16[32,24,128]{2,1,0:T(8,128)(2,1)}), bf16[32,24,128]{2,1,0:T(8,128)(2,1)S(1)}, u32[]{:S(2)}, u32[]{:S(2)}) async-start(bf16[32,24,128]{2,1,0:T(8,128)(2,1)} %reduce_sum.118), calls=%async_computation.3 | async-start | bytes 393216 | tf_op jit(solution)/shard_map/all_to_all | solution.py:62
  233.9 9.7 %all-to-all-done.3 = bf16[32,24,128]{2,1,0:T(8,128)(2,1)S(1)} async-done(((bf16[32,24,128]{2,1,0:T(8,128)(2,1)}), bf16[32,24,128]{2,1,0:T(8,128)(2,1)S(1)}, u32[]{:S(2)}, u32[]{:S(2)}) %all-to-all-start.3) | async-done | bytes 196640 | tf_op jit(solution)/shard_map/all_to_all | solution.py:62
  243.6 1.3 gather_fusion.1
  245.6 14.9 %all_to_all.28 = f32[16,1,512]{2,1,0:T(1,128)S(1)} all-to-all(f32[16,1,512]{2,1,0:T(1,128)S(1)} %broadcast_in_dim.16), channel_id=1, replica_groups=mesh['sp'=32,'tp'=16] {'tp'}, dimensions={0} | all-to-all | bytes 65536 | tf_op jit(solution)/shard_map/all_to_all | solution.py:18
  260.6 0.8 add_convert_fusion
  (68 shorter events, 2.8 us)
Async XLA Ops:
  6.5 125.8 %copy-start = (bf16[1,384,2048]{2,1,0:T(8,128)(2,1)S(1)}, bf16[1,384,2048]{2,1,0:T(8,128)(2,1)}, u32[]{:S(2)}) copy-start(bf16[1,384,2048]{2,1,0:T(8,128)(2,1)} %param.31) | copy-start | bytes 4718596
  6.5 21.1 %copy-start.2 = (bf16[256,128]{1,0:T(8,128)(2,1)S(1)}, bf16[256,128]{1,0:T(8,128)(2,1)}, u32[]{:S(2)}) copy-start(bf16[256,128]{1,0:T(8,128)(2,1)} %param.20) | copy-start | bytes 196612
  7.4 18.9 %collective-permute-start.2 = (bf16[128,128]{1,0:T(8,128)(2,1)S(1)}, bf16[128,128]{1,0:T(8,128)(2,1)S(1)}, u32[]{:S(2)}, u32[]{:S(2)}) collective-permute-start(bf16[128,128]{1,0:T(8,128)(2,1)S(1)} %slice.30), channel_id=1, source_target_pairs={{0,16},{16,32},{32,48},{48,64},{64,80},{80,96},{96,112},{112,128},... | collective-permute-start | bytes 98312 | tf_op jit(solution)/shard_map/ppermute | solution.py:39
  12.0 13.5 %collective-permute-start.1 = (bf16[128]{0:T(256)(128)(2,1)S(1)}, bf16[128]{0:T(256)(128)(2,1)S(1)}, u32[]{:S(2)}, u32[]{:S(2)}) collective-permute-start(bf16[128]{0:T(256)(128)(2,1)S(1)} %slice.29), channel_id=1, source_target_pairs={{0,16},{16,32},{32,48},{48,64},{64,80},{80,96},{96,112},{112,128},... | collective-permute-start | bytes 776 | tf_op jit(solution)/shard_map/ppermute | solution.py:39
  15.9 11.7 %collective-permute-start = (bf16[128,128]{1,0:T(8,128)(2,1)S(1)}, bf16[128,128]{1,0:T(8,128)(2,1)S(1)}, u32[]{:S(2)}, u32[]{:S(2)}) collective-permute-start(bf16[128,128]{1,0:T(8,128)(2,1)S(1)} %slice.28), channel_id=1, source_target_pairs={{0,16},{16,32},{32,48},{48,64},{64,80},{80,96},{96,112},{112,128},... | collective-permute-start | bytes 98312 | tf_op jit(solution)/shard_map/ppermute | solution.py:39
  27.5 21.0 %copy-start.8 = (bf16[1024,128]{1,0:T(8,128)(2,1)S(1)}, bf16[1024,128]{1,0:T(8,128)(2,1)}, u32[]{:S(2)}) copy-start(bf16[1024,128]{1,0:T(8,128)(2,1)} %param.24) | copy-start | bytes 786436
  27.5 21.0 %copy-start.9 = (bf16[256,128]{1,0:T(8,128)(2,1)S(1)}, bf16[256,128]{1,0:T(8,128)(2,1)}, u32[]{:S(2)}) copy-start(bf16[256,128]{1,0:T(8,128)(2,1)} %param.17) | copy-start | bytes 196612
  27.5 21.0 %copy-start.10 = (f32[1024]{0:T(1024)S(1)}, f32[1024]{0:T(1024)}, u32[]{:S(2)}) copy-start(f32[1024]{0:T(1024)} %param.23) | copy-start | bytes 12292
  27.9 33.9 %copy-start.3 = (f32[128]{0:T(128)S(1)}, f32[128]{0:T(128)}, u32[]{:S(2)}) copy-start(f32[128]{0:T(128)} %param.26) | copy-start | bytes 1540
  28.0 33.8 %copy-start.4 = (f32[128]{0:T(128)S(1)}, f32[128]{0:T(128)}, u32[]{:S(2)}) copy-start(f32[128]{0:T(128)} %param.25) | copy-start | bytes 1540
  49.9 11.9 %all-to-all-start = ((f32[16,1,512]{2,1,0:T(1,128)}), f32[16,1,512]{2,1,0:T(1,128)S(1)}, u32[]{:S(2)}, u32[]{:S(2)}) async-start(f32[16,1,512]{2,1,0:T(1,128)} %broadcast_in_dim.13), calls=%async_computation | async-start | bytes 65536 | tf_op jit(solution)/shard_map/all_to_all | solution.py:18
  54.4 72.7 %all-gather.3.cloned.1.call-start = ((), (), s32[]{:S(2)}) async-start(), calls=%async_computation.5 | async-start | bytes 3342336 | tf_op jit(solution)/shard_map/all_gather | solution.py:152
  127.1 5.3 %copy-start.7 = (bf16[1,2048,384]{2,1,0:T(8,128)(2,1)S(1)}, bf16[1,2048,384]{2,1,0:T(8,128)(2,1)}, u32[]{:S(2)}) copy-start(bf16[1,2048,384]{2,1,0:T(8,128)(2,1)} %param.30) | copy-start | bytes 4718596
  145.2 4.6 %copy-start.1 = (f32[256,2]{0,1:T(2,128)S(1)}, f32[256,2]{0,1:T(2,128)}, u32[]{:S(2)}) copy-start(f32[256,2]{0,1:T(2,128)} %param.28) | copy-start | bytes 6148
  145.2 75.7 %all-to-all-start.2 = ((bf16[32,24,16,128]{3,1,0,2:T(8,128)(2,1)}), bf16[32,24,16,128]{3,1,0,2:T(8,128)(2,1)}, u32[]{:S(2)}, u32[]{:S(2)}) async-start(bf16[32,24,16,128]{3,1,0,2:T(8,128)(2,1)} %copy.42), calls=%async_computation.2 | async-start | bytes 6291456 | tf_op jit(solution)/shard_map/all_to_all | solution.py:60
  223.9 36.6 %copy-start.5 = (f32[128]{0:T(128)S(1)}, f32[128]{0:T(128)}, u32[]{:S(2)}) copy-start(f32[128]{0:T(128)} %param.33) | copy-start | bytes 1540
  223.9 36.6 %copy-start.6 = (f32[128]{0:T(128)S(1)}, f32[128]{0:T(128)}, u32[]{:S(2)}) copy-start(f32[128]{0:T(128)} %param.32) | copy-start | bytes 1540
  223.9 19.6 %all-to-all-start.3 = ((bf16[32,24,128]{2,1,0:T(8,128)(2,1)}), bf16[32,24,128]{2,1,0:T(8,128)(2,1)S(1)}, u32[]{:S(2)}, u32[]{:S(2)}) async-start(bf16[32,24,128]{2,1,0:T(8,128)(2,1)} %reduce_sum.118), calls=%async_computation.3 | async-start | bytes 393216 | tf_op jit(solution)/shard_map/all_to_all | solution.py:62
Sparse Core Ops, SparseCore 0:
  87.3 39.7 all-gather.2
where the time goes:
time: 269 us; the launch traced here: 268 us
  waiting for transfers between devices  128 us (48%)
  blocking collectives  58.5 us (22%)
  starting transfers between devices  28.7 us (11%)
  local copies, waits for them, and re-layouts  15.2 us (6%)
  matrix products  14.8 us (6%)
  between operations  14.4 us (5%)
  other arithmetic  8.54 us (3%)
    all_to_all x1, waiting for transfers between devices, expert_rows(): lax.all_to_all(pieces, 'tp', split_axis=2, concat_axis=2, tiled=True)  71.1 us
    all_gather x1, waiting for transfers between devices, local(): lax.all_gather(lax.all_to_all(outgoing, 'sp', split_axis=0, concat_axis=0...  39.9 us
    all_to_all x1, blocking collectives, local(): lax.all_to_all(outgoing, 'sp', split_axis=0, concat_axis=0, tiled=True)  23.3 us
    all_gather x1, blocking collectives, local(): lax.all_gather(attended, 'tp', axis=1, tiled=True).astype(jnp.float32)  20.4 us
    all_to_all x1, blocking collectives, sent_to_all(): lax.all_to_all(jnp.broadcast_to(value[None], (length, *value.shape)), axi...  14.9 us
    ppermute x3, starting transfers between devices, shifted(): return lax.ppermute(block, axis, route)  9.84 us
    all_to_all x1, starting transfers between devices, expert_rows(): lax.all_to_all(summed.astype(jnp.bfloat16), 'sp', split_axis=0, concat_ax...  9.73 us
    all_to_all x1, waiting for transfers between devices, expert_rows(): lax.all_to_all(summed.astype(jnp.bfloat16), 'sp', split_axis=0, concat_ax...  9.68 us
  transfers between devices with their start and end apart: 7, of which 4 were waited for; matrix products, arithmetic and copies ran while one was open for 4% of the time, Pallas kernels for 0%

commit v1 on v0

--- a/solution.py
+++ b/solution.py
@@ -149,11 +149,17 @@
     owner = jnp.arange(tokens * TOP, dtype=jnp.int32) // TOP
     table = jnp.full((expert_count * capacity,), tokens, jnp.int32).at[target].set(owner)
     outgoing = pack_rows(hidden_rows, table, expert_count, capacity)
-    joined = lax.all_gather(
-        lax.all_to_all(outgoing, "sp", split_axis=0, concat_axis=0, tiled=True),
-        "tp",
+    joined = jnp.concatenate(
+        lax.all_to_all(
+            jnp.stack(
+                [lax.all_to_all(outgoing, "sp", split_axis=0, concat_axis=0, tiled=True)]
+                * lax.axis_size("tp")
+            ),
+            "tp",
+            0,
+            0,
+        ),
         axis=2,
-        tiled=True,
     )
     returned = expert_rows(joined, gate_weight, up_weight, down_weight)
     picked = (

time: 269 us -> 290 us (1.078)
  blocking collectives: 58.5 us -> 136 us
  waiting for transfers between devices: 128 us -> 86.9 us
  between operations: 14.4 us -> 1.04 us
  local copies, waits for them, and re-layouts: 15.2 us -> 21.1 us
  starting transfers between devices: 28.7 us -> 22.8 us
    all_to_all x0 -> x1, blocking collectives: none -> 77.8 us  [local(): lax.all_to_all(jnp.stack([lax.all_to_all(outgoing, 'sp', split_axis=0, co...]
    all_gather x1 -> x0, waiting for transfers between devices: 39.9 us -> none  [local(): lax.all_gather(lax.all_to_all(outgoing, 'sp', split_axis=0, concat_axis=0...]
    all_to_all x1, starting transfers between devices: 9.73 us -> 4 us  [expert_rows(): lax.all_to_all(summed.astype(jnp.bfloat16), 'sp', split_axis=0, concat_ax...]
    reshape x0 -> x1, local copies, waits for them, and re-layouts: none -> 3.64 us  [local(): jnp.concatenate(lax.all_to_all(jnp.stack([lax.all_to_all(outgoing, 'sp',...]
  transfers between devices with their start and end apart: 7 -> 6, of which waited for: 4 -> 3; matrix products, arithmetic and copies ran while one was open for 4% -> 3% of each run, Pallas kernels for 0% -> 0%
where the time goes in v1:
time: 290 us; the launch traced here: 289 us
  blocking collectives  136 us (47%)
  waiting for transfers between devices  86.9 us (30%)
  starting transfers between devices  22.8 us (8%)
  local copies, waits for them, and re-layouts  21.1 us (7%)
  matrix products  12.3 us (4%)
  other arithmetic  8.54 us (3%)
    all_to_all x1, blocking collectives, local(): lax.all_to_all(jnp.stack([lax.all_to_all(outgoing, 'sp', split_axis=0, co...  77.8 us
    all_to_all x1, waiting for transfers between devices, expert_rows(): lax.all_to_all(pieces, 'tp', split_axis=2, concat_axis=2, tiled=True)  69.7 us
    all_to_all x1, blocking collectives, local(): lax.all_to_all(outgoing, 'sp', split_axis=0, concat_axis=0, tiled=True)  23.2 us
    all_gather x1, blocking collectives, local(): lax.all_gather(attended, 'tp', axis=1, tiled=True).astype(jnp.float32)  20.4 us
    all_to_all x1, blocking collectives, sent_to_all(): lax.all_to_all(jnp.broadcast_to(value[None], (length, *value.shape)), axi...  15 us
    ppermute x3, starting transfers between devices, shifted(): return lax.ppermute(block, axis, route)  9.84 us
    all_to_all x1, waiting for transfers between devices, expert_rows(): lax.all_to_all(summed.astype(jnp.bfloat16), 'sp', split_axis=0, concat_ax...  9.78 us
    all_to_all x1, waiting for transfers between devices, sent_to_all(): lax.all_to_all(jnp.broadcast_to(value[None], (length, *value.shape)), axi...  7.38 us
  transfers between devices with their start and end apart: 6, of which 3 were waited for; matrix products, arithmetic and copies ran while one was open for 3% of the time, Pallas kernels for 0%

profile of v1, /device:TPU:1, one launch (start us, length us, event | category | flops | bytes accessed | tf_op | source)
XLA Modules:
  0.0 289.1 jit_solution(8624790257206008477)
XLA Ops:
  0.0 0.9 slice.30
  0.9 3.9 %collective-permute-start.2 = (bf16[128,128]{1,0:T(8,128)(2,1)S(1)}, bf16[128,128]{1,0:T(8,128)(2,1)S(1)}, u32[]{:S(2)}, u32[]{:S(2)}) collective-permute-start(bf16[128,128]{1,0:T(8,128)(2,1)S(1)} %slice.30), channel_id=1, source_target_pairs={{0,16},{16,32},{32,48},{48,64},{64,80},{80,96},{96,112},{112,128},... | collective-permute-start | bytes 98312 | tf_op jit(solution)/shard_map/ppermute | solution.py:39
  4.8 0.7 convert.5
  5.5 3.1 %collective-permute-start.1 = (bf16[128]{0:T(256)(128)(2,1)S(1)}, bf16[128]{0:T(256)(128)(2,1)S(1)}, u32[]{:S(2)}, u32[]{:S(2)}) collective-permute-start(bf16[128]{0:T(256)(128)(2,1)S(1)} %slice.29), channel_id=1, source_target_pairs={{0,16},{16,32},{32,48},{48,64},{64,80},{80,96},{96,112},{112,128},... | collective-permute-start | bytes 776 | tf_op jit(solution)/shard_map/ppermute | solution.py:39
  8.6 0.8 slice.28
  9.4 2.8 collective-permute-start
  12.3 0.8 copy.41
  13.4 0.7 broadcast_multiply_fusion
  14.1 1.2 reduce-window.6
  15.9 2.4 scatter_custom_fusion
  19.1 0.7 pad_add_fusion
  19.8 1.2 fusion.65
  21.4 20.4 %all-gather = bf16[256,1,1024]{0,2,1:T(8,128)(2,1)S(1)} all-gather(bf16[256,1,64]{0,2,1:T(8,128)(2,1)S(1)} %fusion.22), channel_id=2, replica_groups=mesh['sp'=32,'tp'=16] {'tp'}, dimensions={2}, use_global_device_ids=true | all-gather | bytes 557056 | tf_op jit(solution)/shard_map/all_gather | solution.py:133
  43.3 4.5 %all-to-all-start = ((f32[16,1,512]{2,1,0:T(1,128)}), f32[16,1,512]{2,1,0:T(1,128)S(1)}, u32[]{:S(2)}, u32[]{:S(2)}) async-start(f32[16,1,512]{2,1,0:T(1,128)} %broadcast_in_dim.13), calls=%async_computation | async-start | bytes 65536 | tf_op jit(solution)/shard_map/all_to_all | solution.py:18
  47.8 7.4 %all-to-all-done = f32[16,1,512]{2,1,0:T(1,128)S(1)} async-done(((f32[16,1,512]{2,1,0:T(1,128)}), f32[16,1,512]{2,1,0:T(1,128)S(1)}, u32[]{:S(2)}, u32[]{:S(2)}) %all-to-all-start) | async-done | bytes 32800 | tf_op jit(solution)/shard_map/all_to_all | solution.py:18
  55.4 1.9 gather_fusion
  57.3 23.2 %all_to_all.32 = bf16[32,24,128]{2,1,0:T(8,128)(2,1)S(1)} all-to-all(bf16[32,24,128]{2,1,0:T(8,128)(2,1)S(1)} %bitcast.86), channel_id=1, replica_groups=mesh['sp'=32,'tp'=16] {'sp'}, dimensions={0} | all-to-all | bytes 393216 | tf_op jit(solution)/shard_map/all_to_all | solution.py:155
  81.1 77.8 %all_to_all.33 = bf16[16,32,24,128]{3,2,1,0:T(8,128)(2,1)S(1)} all-to-all(bf16[16,32,24,128]{3,2,1,0:T(8,128)(2,1)S(1)} %stack.2), channel_id=1, replica_groups=mesh['sp'=32,'tp'=16] {'tp'}, dimensions={0} | all-to-all | bytes 6291456 | tf_op jit(solution)/shard_map/all_to_all | solution.py:153
  158.9 3.6 %copy.44 = bf16[32,24,16,128]{3,2,1,0:T(8,128)(2,1)S(1)} copy(bf16[32,24,16,128]{3,1,0,2:T(8,128)(2,1)S(1)} %bitcast.81) | data formatting | bytes 6291456 | tf_op jit(solution)/shard_map/reshape | solution.py:152
  162.6 1.7 copy-done.1
  164.2 2.8 fusion.2
  167.1 7.4 %fusion.6 = bf16[96,8,16,128]{3,1,2,0:T(8,128)(2,1)} fusion(bf16[1,384,2048]{2,1,0:T(8,128)(2,1)S(1)} %copy-done, bf16[1,2048,384]{2,1,0:T(8,128)(2,1)S(1)} %copy-done.9, bf16[96,8,16,128]{3,2,1,0:T(8,128)(2,1)} %bitcast.85, f32[768,384]{1,0:T(8,128)} %fusion.2), kind=kOutput, calls=%fused_computation.10 | convolution fusion | flops 2419261440 | bytes 10616832 | tf_op jit(solution)/shard_map/dot_general | solution.py:55
  174.4 2.9 %copy.55 = bf16[96,8,16,128]{3,2,1,0:T(8,128)(2,1)S(1)} copy(bf16[96,8,16,128]{3,1,2,0:T(8,128)(2,1)} %fusion.6) | data formatting | bytes 6291456
  177.3 2.5 copy.45
  179.9 4.5 %all-to-all-start.3 = ((bf16[32,24,16,128]{3,1,0,2:T(8,128)(2,1)}), bf16[32,24,16,128]{3,1,0,2:T(8,128)(2,1)}, u32[]{:S(2)}, u32[]{:S(2)}) async-start(bf16[32,24,16,128]{3,1,0,2:T(8,128)(2,1)} %copy.45), calls=%async_computation.3 | async-start | bytes 6291456 | tf_op jit(solution)/shard_map/all_to_all | solution.py:60
  184.4 69.7 %all-to-all-done.3 = bf16[32,24,16,128]{3,1,0,2:T(8,128)(2,1)} async-done(((bf16[32,24,16,128]{3,1,0,2:T(8,128)(2,1)}), bf16[32,24,16,128]{3,1,0,2:T(8,128)(2,1)}, u32[]{:S(2)}, u32[]{:S(2)}) %all-to-all-start.3) | async-done | bytes 3145760 | tf_op jit(solution)/shard_map/all_to_all | solution.py:60
  254.1 3.1 %reduce_sum.118 = bf16[32,24,128]{2,1,0:T(8,128)(2,1)} reduce(bf16[32,24,16,128]{3,1,0,2:T(8,128)(2,1)} %all-to-all-done.3, bf16[]{:T(256)} %constant.87.clone.1), dimensions={2}, to_apply=%region_12.13 | reduce | flops 1474560 | bytes 3342338 | tf_op jit(solution)/shard_map/reduce_sum | solution.py:61
  257.2 4.0 %all-to-all-start.4 = ((bf16[32,24,128]{2,1,0:T(8,128)(2,1)}), bf16[32,24,128]{2,1,0:T(8,128)(2,1)S(1)}, u32[]{:S(2)}, u32[]{:S(2)}) async-start(bf16[32,24,128]{2,1,0:T(8,128)(2,1)} %reduce_sum.118), calls=%async_computation.4 | async-start | bytes 393216 | tf_op jit(solution)/shard_map/all_to_all | solution.py:62
  261.4 9.8 %all-to-all-done.4 = bf16[32,24,128]{2,1,0:T(8,128)(2,1)S(1)} async-done(((bf16[32,24,128]{2,1,0:T(8,128)(2,1)}), bf16[32,24,128]{2,1,0:T(8,128)(2,1)S(1)}, u32[]{:S(2)}, u32[]{:S(2)}) %all-to-all-start.4) | async-done | bytes 196640 | tf_op jit(solution)/shard_map/all_to_all | solution.py:62
  271.2 1.3 gather_fusion.1
  273.2 15.0 %all_to_all.34 = f32[16,1,512]{2,1,0:T(1,128)S(1)} all-to-all(f32[16,1,512]{2,1,0:T(1,128)S(1)} %broadcast_in_dim.16), channel_id=1, replica_groups=mesh['sp'=32,'tp'=16] {'tp'}, dimensions={0} | all-to-all | bytes 65536 | tf_op jit(solution)/shard_map/all_to_all | solution.py:18
  288.3 0.8 add_convert_fusion
  (72 shorter events, 4.7 us)
Async XLA Ops:
  0.0 167.1 %copy-start = (bf16[1,384,2048]{2,1,0:T(8,128)(2,1)S(1)}, bf16[1,384,2048]{2,1,0:T(8,128)(2,1)}, u32[]{:S(2)}) copy-start(bf16[1,384,2048]{2,1,0:T(8,128)(2,1)} %param.31) | copy-start | bytes 4718596
  0.0 21.1 %copy-start.3 = (bf16[256,128]{1,0:T(8,128)(2,1)S(1)}, bf16[256,128]{1,0:T(8,128)(2,1)}, u32[]{:S(2)}) copy-start(bf16[256,128]{1,0:T(8,128)(2,1)} %param.20) | copy-start | bytes 196612
  0.9 18.9 %collective-permute-start.2 = (bf16[128,128]{1,0:T(8,128)(2,1)S(1)}, bf16[128,128]{1,0:T(8,128)(2,1)S(1)}, u32[]{:S(2)}, u32[]{:S(2)}) collective-permute-start(bf16[128,128]{1,0:T(8,128)(2,1)S(1)} %slice.30), channel_id=1, source_target_pairs={{0,16},{16,32},{32,48},{48,64},{64,80},{80,96},{96,112},{112,128},... | collective-permute-start | bytes 98312 | tf_op jit(solution)/shard_map/ppermute | solution.py:39
  5.5 13.5 %collective-permute-start.1 = (bf16[128]{0:T(256)(128)(2,1)S(1)}, bf16[128]{0:T(256)(128)(2,1)S(1)}, u32[]{:S(2)}, u32[]{:S(2)}) collective-permute-start(bf16[128]{0:T(256)(128)(2,1)S(1)} %slice.29), channel_id=1, source_target_pairs={{0,16},{16,32},{32,48},{48,64},{64,80},{80,96},{96,112},{112,128},... | collective-permute-start | bytes 776 | tf_op jit(solution)/shard_map/ppermute | solution.py:39
  9.4 11.7 %collective-permute-start = (bf16[128,128]{1,0:T(8,128)(2,1)S(1)}, bf16[128,128]{1,0:T(8,128)(2,1)S(1)}, u32[]{:S(2)}, u32[]{:S(2)}) collective-permute-start(bf16[128,128]{1,0:T(8,128)(2,1)S(1)} %slice.28), channel_id=1, source_target_pairs={{0,16},{16,32},{32,48},{48,64},{64,80},{80,96},{96,112},{112,128},... | collective-permute-start | bytes 98312 | tf_op jit(solution)/shard_map/ppermute | solution.py:39
  21.0 21.0 %copy-start.10 = (bf16[1024,128]{1,0:T(8,128)(2,1)S(1)}, bf16[1024,128]{1,0:T(8,128)(2,1)}, u32[]{:S(2)}) copy-start(bf16[1024,128]{1,0:T(8,128)(2,1)} %param.24) | copy-start | bytes 786436
  21.0 21.0 %copy-start.11 = (bf16[256,128]{1,0:T(8,128)(2,1)S(1)}, bf16[256,128]{1,0:T(8,128)(2,1)}, u32[]{:S(2)}) copy-start(bf16[256,128]{1,0:T(8,128)(2,1)} %param.17) | copy-start | bytes 196612
  21.0 21.0 %copy-start.12 = (f32[1024]{0:T(1024)S(1)}, f32[1024]{0:T(1024)}, u32[]{:S(2)}) copy-start(f32[1024]{0:T(1024)} %param.23) | copy-start | bytes 12292
  21.4 33.8 %copy-start.4 = (f32[128]{0:T(128)S(1)}, f32[128]{0:T(128)}, u32[]{:S(2)}) copy-start(f32[128]{0:T(128)} %param.26) | copy-start | bytes 1540
  21.4 33.8 %copy-start.5 = (f32[128]{0:T(128)S(1)}, f32[128]{0:T(128)}, u32[]{:S(2)}) copy-start(f32[128]{0:T(128)} %param.25) | copy-start | bytes 1540
  43.3 11.9 %all-to-all-start = ((f32[16,1,512]{2,1,0:T(1,128)}), f32[16,1,512]{2,1,0:T(1,128)S(1)}, u32[]{:S(2)}, u32[]{:S(2)}) async-start(f32[16,1,512]{2,1,0:T(1,128)} %broadcast_in_dim.13), calls=%async_computation | async-start | bytes 65536 | tf_op jit(solution)/shard_map/all_to_all | solution.py:18
  158.9 5.3 %copy-start.8 = (bf16[1,2048,384]{2,1,0:T(8,128)(2,1)S(1)}, bf16[1,2048,384]{2,1,0:T(8,128)(2,1)}, u32[]{:S(2)}) copy-start(bf16[1,2048,384]{2,1,0:T(8,128)(2,1)} %param.29) | copy-start | bytes 4718596
  162.6 1.7 copy-start.1
  164.2 2.8 copy-start.9
  179.9 4.5 %copy-start.2 = (f32[256,2]{0,1:T(2,128)S(1)}, f32[256,2]{0,1:T(2,128)}, u32[]{:S(2)}) copy-start(f32[256,2]{0,1:T(2,128)} %param.28) | copy-start | bytes 6148
  179.9 74.3 %all-to-all-start.3 = ((bf16[32,24,16,128]{3,1,0,2:T(8,128)(2,1)}), bf16[32,24,16,128]{3,1,0,2:T(8,128)(2,1)}, u32[]{:S(2)}, u32[]{:S(2)}) async-start(bf16[32,24,16,128]{3,1,0,2:T(8,128)(2,1)} %copy.45), calls=%async_computation.3 | async-start | bytes 6291456 | tf_op jit(solution)/shard_map/all_to_all | solution.py:60
  257.2 31.1 %copy-start.6 = (f32[128]{0:T(128)S(1)}, f32[128]{0:T(128)}, u32[]{:S(2)}) copy-start(f32[128]{0:T(128)} %param.33) | copy-start | bytes 1540
  257.2 31.1 %copy-start.7 = (f32[128]{0:T(128)S(1)}, f32[128]{0:T(128)}, u32[]{:S(2)}) copy-start(f32[128]{0:T(128)} %param.32) | copy-start | bytes 1540
  257.2 14.0 %all-to-all-start.4 = ((bf16[32,24,128]{2,1,0:T(8,128)(2,1)}), bf16[32,24,128]{2,1,0:T(8,128)(2,1)S(1)}, u32[]{:S(2)}, u32[]{:S(2)}) async-start(bf16[32,24,128]{2,1,0:T(8,128)(2,1)} %reduce_sum.118), calls=%async_computation.4 | async-start | bytes 393216 | tf_op jit(solution)/shard_map/all_to_all | solution.py:62
